TPU v7x, 32 devices: a whole 2x2x4 slice. The times are simulated.
32 devices in a mesh: sp: 8 (over z, y), tp: 4 (over x, core).
Axes of the slice: x: 2, y: 2, z: 4, core: 2. Of those that a mesh axis runs over, the one named last changes fastest.
Arguments:
- tokens: bfloat16 [2048, 2048], P(('sp', 'tp')), may hold values from -16 to 16
- w_query: bfloat16 [2048, 1024], P(None, 'tp'), may hold values from -1 to 1
- w_key: bfloat16 [2048, 256], P(None, 'tp'), may hold values from -1 to 1
- w_value: bfloat16 [2048, 256], P(None, 'tp'), may hold values from -0.125 to 0.125
- w_gate: bfloat16 [2048, 16], P(None, 'tp'), may hold values from -0.125 to 0.125
- gate_bias: float32 [16], P('tp'), as said below
- w_output: bfloat16 [1024, 2048], P('tp'), may hold values from -0.1875 to 0.1875
Outputs:
- mixed: bfloat16 [2048, 2048], P(('sp', 'tp'))
Inputs may be any that keep to these rules, and one draw needn't show every extreme that they name: `gate_bias`: each head's forget gate bias is 4 or more; there is no upper bound.
All inputs are finite; a program needn't handle non-finite values.
Results may differ from a plain program's by a relative error of at most 0.012.
The roundings to bfloat16 on the way count: a program that leaves them out, or rounds other values in their place, can miss the bound.
Values may be sent and summed in bfloat16 or wider, within the bound.
A program may use at most 64 MiB of HBM per device.

v0:
```python
import math
import jax
import jax.numpy as jnp
from jax import lax
from jax.sharding import PartitionSpec as P

HEAD = 64
masked_value = -1e30


def softmax_update(
    carry_state,
    query_here,
    query_cumul,
    query_position,
    key_here,
    value_here,
    key_cumul,
    key_position,
):
    row_peak, row_mass, row_accum = carry_state
    scores = jnp.einsum(
        "kgtd,skd->kgts", query_here, key_here, preferred_element_type=jnp.float32
    ) * HEAD ** (-0.5)
    scores = scores + query_cumul[:, :, :, None] - key_cumul[:, :, None, :]
    allowed = key_position[None, :] <= query_position[:, None]
    scores = jnp.where(allowed, scores, masked_value)
    new_peak = jnp.maximum(row_peak, jnp.max(scores, axis=3))
    weights = jnp.where(allowed, jnp.exp(scores - new_peak[:, :, :, None]), 0.0)
    rescale = jnp.exp(row_peak - new_peak)
    row_mass = row_mass * rescale + jnp.sum(weights, axis=3)
    row_accum = row_accum * rescale[:, :, :, None] + jnp.einsum(
        "kgts,skd->kgtd",
        weights.astype(jnp.bfloat16),
        value_here,
        preferred_element_type=jnp.float32,
    )
    return (new_peak, row_mass, row_accum)


def shards(tokens, w_query, w_key, w_value, w_gate, gate_bias, w_output):
    sp_count = lax.axis_size("sp")
    sp_rank = lax.axis_index("sp")
    query_cols = w_query.shape[1]
    key_cols = w_key.shape[1]
    heads_here = w_gate.shape[1]
    kv_heads_here = key_cols // HEAD
    group_size = heads_here // kv_heads_here
    joined = jnp.concatenate([w_query, w_key, w_value, w_gate], axis=1)
    projected = jnp.dot(
        lax.all_gather(tokens, "tp", axis=0, tiled=True), joined, preferred_element_type=jnp.float32
    ).astype(jnp.bfloat16)
    local_rows = projected.shape[0]
    half_rows = local_rows // 2
    second_block = 2 * sp_rank + 1
    own_gates = jax.nn.log_sigmoid(
        projected[:, query_cols + 2 * key_cols :].astype(jnp.float32) + gate_bias
    )
    totals = jnp.sum(own_gates.reshape(2, half_rows, heads_here), axis=1)
    all_totals = lax.all_gather(totals[None], "sp", axis=0, tiled=True)
    ordered = all_totals.reshape(2 * sp_count, heads_here)
    prefix_sums = jnp.cumsum(ordered, axis=0) - ordered
    queries = (
        projected[:, :query_cols]
        .reshape(2, half_rows, kv_heads_here, group_size, HEAD)
        .transpose(0, 2, 3, 1, 4)
    )
    query_blocks = (2 * sp_rank, second_block)
    query_cumul = []
    query_position = []
    for side_index in range(2):
        base_value = lax.dynamic_index_in_dim(
            prefix_sums, query_blocks[side_index], 0, keepdims=False
        )
        cumul_rows = base_value[None, :] + jnp.cumsum(
            own_gates[side_index * half_rows : (side_index + 1) * half_rows], axis=0
        )
        query_cumul.append(
            cumul_rows.reshape(half_rows, kv_heads_here, group_size).transpose(1, 2, 0)
        )
        query_position.append(
            query_blocks[side_index] * half_rows + jnp.arange(half_rows, dtype=jnp.int32)
        )
    initial = (
        jnp.full((2, kv_heads_here, group_size, half_rows), masked_value, jnp.float32),
        jnp.zeros((2, kv_heads_here, group_size, half_rows), jnp.float32),
        jnp.zeros((2, kv_heads_here, group_size, half_rows, HEAD), jnp.float32),
    )
    gathered = lax.all_gather(projected[:, query_cols:], "sp", axis=0, tiled=True)
    row_count = gathered.shape[0]
    piece_blocks = row_count // half_rows
    per_step = math.gcd(piece_blocks, max(1, 1024 // half_rows))
    step_rows = per_step * half_rows
    step_count = row_count // step_rows
    first_row = half_rows * jnp.arange(piece_blocks, dtype=jnp.int32)
    owner_rank = first_row // local_rows
    half_index = first_row % local_rows // half_rows
    block_ids = 2 * owner_rank + half_index
    gate_logs = jax.nn.log_sigmoid(gathered[:, 2 * key_cols :].astype(jnp.float32) + gate_bias)
    gate_logs = gate_logs.reshape(piece_blocks, half_rows, heads_here)
    base_values = jnp.take(prefix_sums, block_ids, axis=0)
    key_cumul_all = (base_values[:, None, :] + jnp.cumsum(gate_logs, axis=1)).reshape(
        row_count, kv_heads_here, group_size
    )
    key_position_all = (
        block_ids[:, None] * half_rows + jnp.arange(half_rows, dtype=jnp.int32)[None, :]
    ).reshape(row_count)
    earliest = jnp.min(block_ids.reshape(step_count, per_step), axis=1)

    def one_step(step_index, inner_state):
        start_row = step_index * step_rows
        block_rows = lax.dynamic_slice_in_dim(gathered, start_row, step_rows, 0)
        key_here = block_rows[:, :key_cols].reshape(step_rows, kv_heads_here, HEAD)
        value_here = block_rows[:, key_cols : 2 * key_cols].reshape(step_rows, kv_heads_here, HEAD)
        key_cumul = lax.dynamic_slice_in_dim(key_cumul_all, start_row, step_rows, 0).transpose(
            1, 2, 0
        )
        key_position = lax.dynamic_slice_in_dim(key_position_all, start_row, step_rows, 0)
        first_id = earliest[step_index]
        results = []
        for side_index in range(2):
            head_state = tuple((member[side_index] for member in inner_state))

            def compute(head_state, side_index=side_index):
                return softmax_update(
                    head_state,
                    queries[side_index],
                    query_cumul[side_index],
                    query_position[side_index],
                    key_here,
                    value_here,
                    key_cumul,
                    key_position,
                )

            head_state = lax.cond(
                first_id <= query_blocks[side_index],
                compute,
                lambda unchanged: unchanged,
                head_state,
            )
            results.append(head_state)
        return tuple((jnp.stack([results[0][member], results[1][member]]) for member in range(3)))

    row_peak, row_mass, row_accum = lax.fori_loop(0, step_count, one_step, initial)
    attended = (row_accum / row_mass[:, :, :, :, None]).astype(jnp.bfloat16)
    attended = attended.transpose(0, 3, 1, 2, 4).reshape(local_rows, heads_here * HEAD)
    return lax.psum_scatter(
        jnp.dot(attended, w_output, preferred_element_type=jnp.float32).astype(jnp.bfloat16),
        "tp",
        scatter_dimension=0,
        tiled=True,
    )


def solution(mesh):
    return jax.shard_map(
        shards,
        mesh=mesh,
        in_specs=(
            P(("sp", "tp"), None),
            P(None, "tp"),
            P(None, "tp"),
            P(None, "tp"),
            P(None, "tp"),
            P("tp"),
            P("tp", None),
        ),
        out_specs=P(("sp", "tp"), None),
        check_vma=False,
    )
```

profile of v0, /device:TPU:0, one launch (start us, length us, event | category | flops | bytes accessed | tf_op | source)
XLA Modules:
  0.0 130.7 jit_solution(12914409057158961123)
XLA Ops:
  6.5 0.7 all-gather.4.cloned.1.call-update
  7.3 1.0 copy.42
  8.3 1.2 copy.41
  9.6 1.2 copy.40
  11.1 17.2 %all-gather.4.cloned.1.call-done = bf16[256,2048]{1,0:T(8,128)(2,1)} async-done(((bf16[64,2048]{1,0:T(8,128)(2,1)}), bf16[256,2048]{1,0:T(8,128)(2,1)}) %all-gather.4.cloned.1.call-update) | async-done | bytes 1048592 | tf_op jit(solution)/shard_map/all_gather | solution.py:51
  28.3 2.7 %fusion.47 = bf16[256,388]{0,1:T(8,128)(2,1)S(1)} fusion(bf16[256,2048]{1,0:T(8,128)(2,1)} %all-gather.4.cloned.1.call-done, bf16[2048,4]{1,0:T(8,128)(2,1)S(1)} %copy.42, bf16[2048,64]{1,0:T(8,128)(2,1)S(1)} %copy.41, bf16[2048,64]{1,0:T(8,128)(2,1)S(1)} %copy.40, bf16[2048,256]{1,0:T(8,128)(2,1)} %param.14), kind=kOutput, calls=%fused_computation.71 | convolution fusion | flops 413303808 | bytes 2836480 | tf_op jit(solution)/shard_map/dot_general | solution.py:50
  31.2 31.5 %all_gather.10 = bf16[2048,132]{0,1:T(8,128)(2,1)S(1)} all-gather(bf16[256,132]{0,1:T(8,128)(2,1)S(1)} %slice.96), channel_id=1, replica_groups=mesh['sp'=8,'tp'=4] {'sp'}, dimensions={0}, use_global_device_ids=true | all-gather | bytes 608256 | tf_op jit(solution)/shard_map/all_gather | solution.py:89
  62.9 20.5 %all-gather.1 = f32[8,2,4]{2,1,0:T(2,128)S(1)} all-gather(f32[1,2,4]{2,1,0:T(2,128)S(1)} %bitcast.194), channel_id=2, replica_groups=mesh['sp'=8,'tp'=4] {'sp'}, dimensions={0}, use_global_device_ids=true | all-gather | bytes 288 | tf_op jit(solution)/shard_map/all_gather | solution.py:60
  84.1 0.6 gather_fusion
  84.8 1.2 broadcast_add_fusion.2
  85.9 1.6 %copy.45 = f32[16,128,4]{1,0,2:T(8,128)S(1)} copy(f32[16,128,4]{2,0,1:T(8,128)} %broadcast_add_fusion.2) | data formatting | bytes 65536 | tf_op jit(solution)/shard_map/add | solution.py:102
  88.4 9.0 %while.18 = (s32[]{:T(128)}, f32[2,1,4,128]{3,2,1,0:T(4,128)S(1)}, f32[2,1,4,128]{3,2,1,0:T(4,128)S(1)}, f32[2,1,4,128,64]{3,4,2,1,0:T(8,128)S(1)}, s32[2]{0:T(1...) while((s32[]{:T(128)}, f32[2,1,4,128]{3,2,1,0:T(4,128)S(1)}, ...), condition=%wide.region_15.16_spmd.clone, body=%wide.region_6.15_spmd.clone.sunk | while | flops 280433920 | bytes 16568903 | solution.py:145
  88.4 0.7 dynamic_slice.54
  89.9 2.2 %conditional.6 = (f32[1,1,4,128]{3,2,1,0:T(4,128)S(1)}, f32[1,1,4,128]{3,2,1,0:T(4,128)S(1)}, f32[1,1,4,128,64]{3,4,2,1,0:T(8,128)S(1)}) conditional(s32[]{:T(128)} %convert_element_type.63, (f32[1,4,128]{2,1,0:T(4,128)S(1)}, f32[1,4,128]{2,1,0:T(4,128)S(1)}, f32[1,4,128,64]{2,3,1,0:T(8,128)S(1)}) %tuple.137, (s32[1024]{0:T(1024)S(1)}, s32[]{:T(128)}, ...), branch_computations={%region_11.11_spmd, %region_12.14_spmd} | conditional | flops 140183168 | bytes 7460380 | solution.py:136
  90.1 0.8 fusion.60
  90.9 0.6 fusion.21
  91.5 0.6 fusion.23
  92.8 2.2 %conditional.7 = (f32[1,1,4,128]{3,2,1,0:T(4,128)S(1)}, f32[1,1,4,128]{3,2,1,0:T(4,128)S(1)}, f32[1,1,4,128,64]{3,4,2,1,0:T(8,128)S(1)}) conditional(s32[]{:T(128)} %convert_element_type.64, (f32[1,4,128]{2,1,0:T(4,128)S(1)}, f32[1,4,128]{2,1,0:T(4,128)S(1)}, f32[1,4,128,64]{2,3,1,0:T(8,128)S(1)}) %tuple.139, (s32[1024]{0:T(1024)S(1)}, s32[]{:T(128)}, ...), branch_computations={%region_7.7_spmd, %region_8.10_spmd} | conditional | flops 140183168 | bytes 7460380 | solution.py:136
  93.0 0.8 fusion.59
  93.8 0.6 fusion.5
  94.4 0.6 fusion.7
  95.1 0.7 dynamic_slice.54
  97.6 1.5 %convolution_convert_fusion = bf16[256,2048]{1,0:T(8,128)(2,1)} fusion(bf16[256,2048]{1,0:T(8,128)(2,1)S(1)} %copy-done, bf16[32,8,2,128]{3,2,1,0:T(2,128)(2,1)S(1)} %bitcast.184), kind=kOutput, calls=%fused_computation.61 | convolution fusion | flops 268959744 | bytes 2228224 | tf_op jit(solution)/shard_map/dot_general | solution.py:149
  99.1 24.8 %reduce-scatter.2.cloned.1.call-done = bf16[64,2048]{1,0:T(8,128)(2,1)} async-done(((bf16[256,2048]{1,0:T(8,128)(2,1)}), bf16[64,2048]{1,0:T(8,128)(2,1)}) %reduce-scatter.2.cloned.1.call-update) | async-done | bytes 262160 | tf_op jit(solution)/shard_map/reduce_scatter | solution.py:148
  (72 shorter events, 3.0 us)
Async XLA Ops:
  6.5 91.0 %copy-start = (bf16[256,2048]{1,0:T(8,128)(2,1)S(1)}, bf16[256,2048]{1,0:T(8,128)(2,1)}, u32[]{:S(2)}) copy-start(bf16[256,2048]{1,0:T(8,128)(2,1)} %param.19) | copy-start | bytes 3145732
  6.5 21.8 %all-gather.4.cloned.1.call-start = ((), (), s32[]{:S(2)}) async-start(), calls=%async_computation.1 | async-start | bytes 1310720 | tf_op jit(solution)/shard_map/all_gather | solution.py:51
  7.3 116.6 %reduce-scatter.2.cloned.1.call-start = ((), (), s32[]{:S(2)}) async-start(), calls=%async_computation.2 | async-start | bytes 1310720 | tf_op jit(solution)/shard_map/reduce_scatter | solution.py:148
  11.1 20.0 %copy-start.1 = (f32[4]{0:T(128)S(1)}, f32[4]{0:T(128)}, u32[]{:S(2)}) copy-start(f32[4]{0:T(128)} %param.18) | copy-start | bytes 52
Sparse Core Ops, SparseCore 0:
  8.9 19.4 all-gather.3
  99.2 24.6 reduce-scatter.1
where the time goes:
time: 131 us
  blocking collectives  52 us (40%)
  waiting for transfers between devices  42.8 us (33%)
  between operations  13.6 us (10%)
  local copies, waits for them, and re-layouts  8.46 us (6%)
  matrix products  6.94 us (5%)
  other arithmetic  3.82 us (3%)
  loops' own time  3.1 us (2%)
    all_gather x1, blocking collectives, shards(): lax.all_gather(projected[:, query_cols:], 'sp', axis=0, tiled=True)  31.5 us
    reduce_scatter x1, waiting for transfers between devices, shards(): lax.psum_scatter(jnp.dot(attended, w_output, preferred_element_type=jnp.f...  24.8 us
    all_gather x1, blocking collectives, shards(): all_totals = lax.all_gather(totals[None], 'sp', axis=0, tiled=True)  20.5 us
    all_gather x1, waiting for transfers between devices, shards(): lax.all_gather(tokens, 'tp', axis=0, tiled=True)  17.2 us
    unnamed x10, local copies, waits for them, and re-layouts  3.63 us
    another operation x1, loops' own time, shards(): lax.fori_loop(0, step_count, one_step, initial)  3.01 us
    dot_general x1, matrix products, shards(): jnp.dot(lax.all_gather(tokens, 'tp', axis=0, tiled=True), joined, preferr...  2.72 us
  transfers between devices with their start and end apart: 2, of which 2 were waited for; matrix products, arithmetic and copies ran while one was open for 3% of the time, Pallas kernels for 0%

commit v1 on v0

--- a/solution.py
+++ b/solution.py
@@ -6,6 +6,13 @@
 
 HEAD = 64
 masked_value = -1e30
+
+
+def swapped_in(block, axis, dim):
+    size = lax.axis_size(axis)
+    parts = jnp.stack([block for _ in range(size)])
+    parts = lax.all_to_all(parts, axis, split_axis=0, concat_axis=0)
+    return jnp.concatenate(parts, axis=dim)
 
 
 def softmax_update(
@@ -48,7 +55,7 @@
     group_size = heads_here // kv_heads_here
     joined = jnp.concatenate([w_query, w_key, w_value, w_gate], axis=1)
     projected = jnp.dot(
-        lax.all_gather(tokens, "tp", axis=0, tiled=True), joined, preferred_element_type=jnp.float32
+        swapped_in(tokens, "tp", 0), joined, preferred_element_type=jnp.float32
     ).astype(jnp.bfloat16)
     local_rows = projected.shape[0]
     half_rows = local_rows // 2

time: 131 us -> 131 us (level)
  waiting for transfers between devices: 42.8 us -> 36.4 us
  starting transfers between devices: 0.04 us -> 4.24 us
    all_gather x1 -> x0, waiting for transfers between devices: 17.2 us -> none  [shards(): lax.all_gather(tokens, 'tp', axis=0, tiled=True)]
    all_to_all x0 -> x1, waiting for transfers between devices: none -> 11.5 us  [swapped_in(): parts = lax.all_to_all(parts, axis, split_axis=0, concat_axis=0)]
    all_to_all x0 -> x1, starting transfers between devices: none -> 4.24 us  [swapped_in(): parts = lax.all_to_all(parts, axis, split_axis=0, concat_axis=0)]
    another operation x0 -> x1, local copies, waits for them, and re-layouts: none -> 2.16 us  [swapped_in(): parts = jnp.stack([block for _ in range(size)])]
    unnamed x10 -> x14, local copies, waits for them, and re-layouts: 3.63 us -> 2.73 us
  transfers between devices with their start and end apart: 2 -> 2, of which waited for: 2 -> 2; matrix products, arithmetic and copies ran while one was open for 3% -> 2% of each run, Pallas kernels for 0% -> 0%
where the time goes in v1:
time: 131 us
  blocking collectives  53.1 us (41%)
  waiting for transfers between devices  36.4 us (28%)
  between operations  13.6 us (10%)
  local copies, waits for them, and re-layouts  9.72 us (7%)
  matrix products  6.76 us (5%)
  starting transfers between devices  4.24 us (3%)
  other arithmetic  3.82 us (3%)
  loops' own time  3.1 us (2%)
    all_gather x1, blocking collectives, shards(): lax.all_gather(projected[:, query_cols:], 'sp', axis=0, tiled=True)  32.8 us
    reduce_scatter x1, waiting for transfers between devices, shards(): lax.psum_scatter(jnp.dot(attended, w_output, preferred_element_type=jnp.f...  24.8 us
    all_gather x1, blocking collectives, shards(): all_totals = lax.all_gather(totals[None], 'sp', axis=0, tiled=True)  20.3 us
    all_to_all x1, waiting for transfers between devices, swapped_in(): parts = lax.all_to_all(parts, axis, split_axis=0, concat_axis=0)  11.5 us
    all_to_all x1, starting transfers between devices, swapped_in(): parts = lax.all_to_all(parts, axis, split_axis=0, concat_axis=0)  4.24 us
    another operation x1, loops' own time, shards(): lax.fori_loop(0, step_count, one_step, initial)  3.01 us
    unnamed x14, local copies, waits for them, and re-layouts  2.73 us
  transfers between devices with their start and end apart: 2, of which 2 were waited for; matrix products, arithmetic and copies ran while one was open for 2% of the time, Pallas kernels for 0%

profile of v1, /device:TPU:0, one launch (start us, length us, event | category | flops | bytes accessed | tf_op | source)
XLA Modules:
  0.0 130.7 jit_solution(212295692415183427)
XLA Ops:
  6.5 2.2 %stack.106 = bf16[4,64,2048]{2,1,0:T(8,128)(2,1)} broadcast(bf16[64,2048]{1,0:T(8,128)(2,1)} %param.13), dimensions={1,2} | broadcast | bytes 1310720 | tf_op jit(solution)/shard_map/stack | solution.py:13
  8.7 4.2 %all-to-all-start = ((bf16[4,64,2048]{2,1,0:T(8,128)(2,1)}), bf16[4,64,2048]{2,1,0:T(8,128)(2,1)S(1)}, u32[]{:S(2)}, u32[]{:S(2)}) async-start(bf16[4,64,2048]{2,1,0:T(8,128)(2,1)} %stack.106), calls=%async_computation | async-start | bytes 2097152 | tf_op jit(solution)/shard_map/all_to_all | solution.py:14
  12.9 1.1 copy.42
  14.3 1.2 copy.40
  15.8 11.5 %all-to-all-done = bf16[4,64,2048]{2,1,0:T(8,128)(2,1)S(1)} async-done(((bf16[4,64,2048]{2,1,0:T(8,128)(2,1)}), bf16[4,64,2048]{2,1,0:T(8,128)(2,1)S(1)}, u32[]{:S(2)}, u32[]{:S(2)}) %all-to-all-start) | async-done | bytes 1048608 | tf_op jit(solution)/shard_map/all_to_all | solution.py:14
  27.4 2.5 %fusion.47 = bf16[256,388]{0,1:T(8,128)(2,1)S(1)} fusion(bf16[256,2048]{1,0:T(8,128)(2,1)S(1)} %bitcast.183, bf16[2048,4]{1,0:T(8,128)(2,1)} %copy.42, bf16[2048,64]{1,0:T(8,128)(2,1)S(1)} %copy.41, bf16[2048,64]{1,0:T(8,128)(2,1)S(1)} %copy.40, bf16[2048,256]{1,0:T(8,128)(2,1)} %param.14), kind=kOutput, calls=%fused_computation.71 | convolution fusion | flops 413303808 | bytes 2836480 | tf_op jit(solution)/shard_map/dot_general | solution.py:57
  30.1 32.8 %all_gather.6 = bf16[2048,132]{0,1:T(8,128)(2,1)S(1)} all-gather(bf16[256,132]{0,1:T(8,128)(2,1)S(1)} %slice.96), channel_id=1, replica_groups=mesh['sp'=8,'tp'=4] {'sp'}, dimensions={0}, use_global_device_ids=true | all-gather | bytes 608256 | tf_op jit(solution)/shard_map/all_gather | solution.py:96
  63.0 20.3 %all-gather.1 = f32[8,2,4]{2,1,0:T(2,128)S(1)} all-gather(f32[1,2,4]{2,1,0:T(2,128)S(1)} %bitcast.196), channel_id=2, replica_groups=mesh['sp'=8,'tp'=4] {'sp'}, dimensions={0}, use_global_device_ids=true | all-gather | bytes 288 | tf_op jit(solution)/shard_map/all_gather | solution.py:67
  84.0 0.6 gather_fusion
  84.7 1.2 broadcast_add_fusion.2
  85.8 1.6 %copy.45 = f32[16,128,4]{1,0,2:T(8,128)S(1)} copy(f32[16,128,4]{2,0,1:T(8,128)} %broadcast_add_fusion.2) | data formatting | bytes 65536 | tf_op jit(solution)/shard_map/add | solution.py:109
  88.3 9.0 %while.18 = (s32[]{:T(128)}, f32[2,1,4,128]{3,2,1,0:T(4,128)S(1)}, f32[2,1,4,128]{3,2,1,0:T(4,128)S(1)}, f32[2,1,4,128,64]{3,4,2,1,0:T(8,128)S(1)}, s32[2]{0:T(1...) while((s32[]{:T(128)}, f32[2,1,4,128]{3,2,1,0:T(4,128)S(1)}, ...), condition=%wide.region_15.16_spmd.clone, body=%wide.region_6.15_spmd.clone.sunk | while | flops 280433920 | bytes 16568903 | solution.py:152
  88.4 0.7 dynamic_slice.54
  89.8 2.2 %conditional.6 = (f32[1,1,4,128]{3,2,1,0:T(4,128)S(1)}, f32[1,1,4,128]{3,2,1,0:T(4,128)S(1)}, f32[1,1,4,128,64]{3,4,2,1,0:T(8,128)S(1)}) conditional(s32[]{:T(128)} %convert_element_type.63, (f32[1,4,128]{2,1,0:T(4,128)S(1)}, f32[1,4,128]{2,1,0:T(4,128)S(1)}, f32[1,4,128,64]{2,3,1,0:T(8,128)S(1)}) %tuple.137, (s32[1024]{0:T(1024)S(1)}, s32[]{:T(128)}, ...), branch_computations={%region_11.11_spmd, %region_12.14_spmd} | conditional | flops 140183168 | bytes 7460380 | solution.py:143
  90.0 0.8 fusion.60
  90.8 0.6 fusion.21
  91.4 0.6 fusion.23
  92.7 2.2 %conditional.7 = (f32[1,1,4,128]{3,2,1,0:T(4,128)S(1)}, f32[1,1,4,128]{3,2,1,0:T(4,128)S(1)}, f32[1,1,4,128,64]{3,4,2,1,0:T(8,128)S(1)}) conditional(s32[]{:T(128)} %convert_element_type.64, (f32[1,4,128]{2,1,0:T(4,128)S(1)}, f32[1,4,128]{2,1,0:T(4,128)S(1)}, f32[1,4,128,64]{2,3,1,0:T(8,128)S(1)}) %tuple.139, (s32[1024]{0:T(1024)S(1)}, s32[]{:T(128)}, ...), branch_computations={%region_7.7_spmd, %region_8.10_spmd} | conditional | flops 140183168 | bytes 7460380 | solution.py:143
  92.9 0.8 fusion.59
  93.7 0.6 fusion.5
  94.3 0.6 fusion.7
  95.0 0.7 dynamic_slice.54
  97.5 1.5 %convolution_convert_fusion = bf16[256,2048]{1,0:T(8,128)(2,1)} fusion(bf16[256,2048]{1,0:T(8,128)(2,1)S(1)} %copy-done, bf16[32,8,2,128]{3,2,1,0:T(2,128)(2,1)S(1)} %bitcast.186), kind=kOutput, calls=%fused_computation.61 | convolution fusion | flops 268959744 | bytes 2228224 | tf_op jit(solution)/shard_map/dot_general | solution.py:156
  99.0 24.8 %reduce-scatter.2.cloned.1.call-done = bf16[64,2048]{1,0:T(8,128)(2,1)} async-done(((bf16[256,2048]{1,0:T(8,128)(2,1)}), bf16[64,2048]{1,0:T(8,128)(2,1)}) %reduce-scatter.2.cloned.1.call-update) | async-done | bytes 262160 | tf_op jit(solution)/shard_map/reduce_scatter | solution.py:155
  (76 shorter events, 3.2 us)
Async XLA Ops:
  6.5 91.0 %copy-start = (bf16[256,2048]{1,0:T(8,128)(2,1)S(1)}, bf16[256,2048]{1,0:T(8,128)(2,1)}, u32[]{:S(2)}) copy-start(bf16[256,2048]{1,0:T(8,128)(2,1)} %param.19) | copy-start | bytes 3145732
  6.5 6.4 %copy-start.2 = (bf16[2048,4]{0,1:T(4,128)(2,1)S(1)}, bf16[2048,4]{0,1:T(4,128)(2,1)}, u32[]{:S(2)}) copy-start(bf16[2048,4]{0,1:T(4,128)(2,1)} %param.17) | copy-start | bytes 49156
  6.5 7.5 %copy-start.1 = (bf16[2048,64]{0,1:T(8,128)(2,1)S(1)}, bf16[2048,64]{0,1:T(8,128)(2,1)}, u32[]{:S(2)}) copy-start(bf16[2048,64]{0,1:T(8,128)(2,1)} %param.16) | copy-start | bytes 786436
  8.7 18.7 %all-to-all-start = ((bf16[4,64,2048]{2,1,0:T(8,128)(2,1)}), bf16[4,64,2048]{2,1,0:T(8,128)(2,1)S(1)}, u32[]{:S(2)}, u32[]{:S(2)}) async-start(bf16[4,64,2048]{2,1,0:T(8,128)(2,1)} %stack.106), calls=%async_computation | async-start | bytes 2097152 | tf_op jit(solution)/shard_map/all_to_all | solution.py:14
  12.9 110.9 %reduce-scatter.2.cloned.1.call-start = ((), (), s32[]{:S(2)}) async-start(), calls=%async_computation.2 | async-start | bytes 1310720 | tf_op jit(solution)/shard_map/reduce_scatter | solution.py:155
  27.4 2.6 %copy-start.3 = (f32[4]{0:T(128)S(1)}, f32[4]{0:T(128)}, u32[]{:S(2)}) copy-start(f32[4]{0:T(128)} %param.18) | copy-start | bytes 52
Sparse Core Ops, SparseCore 0:
  99.1 24.6 reduce-scatter.1
